TPU v7x, 32 devices: a whole 2x2x4 slice. The times are simulated.
32 devices in a mesh: fs: 8 (over z, y), tp: 4 (over x, core).
Axes of the slice: x: 2, y: 2, z: 4, core: 2. Of those that a mesh axis runs over, the one named last changes fastest.
Arguments:
- tokens: bfloat16 [8192, 2048], P('fs'), may hold values from -6 to 6
- norm_gain: float32 [2048], P('fs'), may hold values from 0.1 to 1.9
- gate_train: float32 [8, 2048, 768], P(None, 'fs', 'tp'), may hold values from -0.125 to 0.125
- up_train: float32 [8, 2048, 768], P(None, 'fs', 'tp'), may hold values from -0.125 to 0.125
- down_train: float32 [8, 768, 2048], P(None, 'fs', 'tp'), may hold values from -0.21875 to 0.21875
- expert_ids: int32 [8192, 2], P('fs'), may hold values from 0 to 7, all different within a row; in each aligned block of 1024 rows (0 to 1023, 1024 to 2047, ...) at most 512 rows name the same one
- route_weights: float32 [8192, 2], P('fs'), may hold values from 0.1 to 1
Outputs:
- gate_serve: bfloat16 [8, 2048, 768], P('fs', None, 'tp')
- up_serve: bfloat16 [8, 2048, 768], P('fs', None, 'tp')
- down_serve: bfloat16 [8, 768, 2048], P('fs', 'tp')
- mixed: bfloat16 [8192, 2048], P('fs', 'tp')
Inputs may be any that keep to these rules, and one draw needn't show every extreme that they name: `expert_ids`: each row names 2 different experts. Within each aligned block of 1024 rows no expert is named more than 512 times, and in every block some expert is named exactly 512 times; every expert is named somewhere.
All inputs are finite; a program needn't handle non-finite values.
Results may differ from a plain program's by a relative error of at most 0.011.
Values may be sent and summed in bfloat16 or wider, within the bound.
A program may use at most 128 MiB of HBM per device.

v0:
```python
import jax
import jax.numpy as jnp
from jax import lax
from jax.sharding import PartitionSpec as P

epsilon = 1e-06


def on_device(tokens, norm_gain, gate_train, up_train, down_train, expert_ids, route_weights):
    experts, rows, cols = gate_train.shape
    fs_at = lax.axis_index("fs")
    tok_rows, picks = expert_ids.shape
    down_rows, down_cols = down_train.shape[1:]
    fs_count = lax.axis_size("fs")
    gate_up = jnp.concatenate(
        [norm_gain[None, :, None] * gate_train, norm_gain[None, :, None] * up_train], axis=2
    ).astype(jnp.bfloat16)
    gate_up = gate_up.transpose(1, 0, 2).reshape(rows, experts * 2 * cols)
    gate_up_all = lax.all_gather(gate_up, "fs", axis=0, tiled=True)
    down_all = lax.all_gather(
        down_train.astype(jnp.bfloat16).reshape(experts * down_rows, down_cols),
        "fs",
        axis=0,
        tiled=True,
    )
    tok_float = tokens.astype(jnp.float32)
    normed = (
        tok_float * lax.rsqrt(jnp.mean(tok_float * tok_float, axis=-1, keepdims=True) + epsilon)
    ).astype(jnp.bfloat16)
    shares = route_weights / jnp.sum(route_weights, axis=-1, keepdims=True)
    group = 2 * lax.axis_size("tp")
    picked = [jnp.zeros((tok_rows, cols), jnp.float32) for _ in range(picks)]
    for first in range(0, experts, group):
        part = gate_up_all[:, first * 2 * cols : (first + group) * 2 * cols]
        if first:
            part, picked = lax.optimization_barrier((part, picked))
        acts = jnp.dot(normed, part, preferred_element_type=jnp.float32)
        for at in range(group):
            g = acts[:, at * 2 * cols : at * 2 * cols + cols]
            u = acts[:, at * 2 * cols + cols : (at + 1) * 2 * cols]
            h = jax.nn.silu(g) * u
            for k in range(picks):
                picked[k] = picked[k] + jnp.where(expert_ids[:, k : k + 1] == first + at, h, 0.0)
    hidden = jnp.stack([picked[k] * shares[:, k : k + 1] for k in range(picks)], 0)
    hidden_all = lax.all_gather(hidden.astype(jnp.bfloat16), "tp", axis=2, tiled=True)
    hidden_all = hidden_all.reshape(picks, tok_rows, fs_count, 1, down_rows)
    ids = jnp.arange(experts, dtype=jnp.int32)[None, None, :, None]
    mixed = jnp.zeros((tok_rows, down_cols), jnp.float32)
    for first in range(0, fs_count, group):
        blocks = hidden_all[:, :, first : first + group]
        if first:
            blocks, mixed = lax.optimization_barrier((blocks, mixed))
        spread = jnp.zeros((tok_rows, group, experts, down_rows), jnp.bfloat16)
        for k in range(picks):
            spread = jnp.where(expert_ids[:, k][:, None, None, None] == ids, blocks[k], spread)
        depth = experts * down_rows
        mixed = mixed + jnp.dot(
            spread.reshape(tok_rows, group * depth),
            down_all[first * depth : (first + group) * depth],
            preferred_element_type=jnp.float32,
        )
    mixed = mixed.astype(jnp.bfloat16)
    own = lax.dynamic_slice_in_dim(gate_up_all, fs_at * 2 * cols, 2 * cols, 1)
    down_own = lax.dynamic_slice_in_dim(
        down_all.reshape(fs_count, experts, down_rows, down_cols), fs_at, 1, 1
    ).reshape(1, fs_count * down_rows, down_cols)
    down_serve = lax.all_to_all(down_own, "tp", split_axis=1, concat_axis=2, tiled=True)
    return (own[None, :, :cols], own[None, :, cols:], down_serve, mixed)


def solution(mesh):
    return jax.shard_map(
        on_device,
        mesh=mesh,
        in_specs=(
            P("fs", None),
            P("fs"),
            P(None, "fs", "tp"),
            P(None, "fs", "tp"),
            P(None, "fs", "tp"),
            P("fs", None),
            P("fs", None),
        ),
        out_specs=(P("fs", None, "tp"), P("fs", None, "tp"), P("fs", "tp", None), P("fs", "tp")),
        check_vma=False,
    )
```

profile of v0, /device:TPU:0, one launch (start us, length us, event | category | flops | bytes accessed | tf_op | source)
XLA Modules:
  0.0 353.5 jit_solution(751838854216082823)
XLA Ops:
  7.2 0.0 all-gather.4.cloned.1.call-start
  7.2 2.3 multiply_convert_fusion.1
  9.6 1.3 pad_maximum_fusion
  10.9 0.0 all-gather.6.cloned.1.call-start
  10.9 1.0 convert_element_type.14
  11.9 0.0 all-gather.8.cloned.1.call-start
  12.0 0.2 compare_reduce_fusion.15
  12.2 3.1 fusion
  15.4 174.5 %all-gather.4.cloned.1.call-done = bf16[2048,3072]{0,1:T(8,128)(2,1)} async-done(((bf16[256,3072]{0,1:T(8,128)(2,1)}), bf16[2048,3072]{0,1:T(8,128)(2,1)}) %all-gather.4.cloned.1.call-update) | async-done | bytes 12582928 | tf_op jit(solution)/shard_map/all_gather | solution.py:19
  189.9 17.1 %fusion.2 = f32[1024,3072]{1,0:T(8,128)S(1)} fusion(bf16[2048,3072]{0,1:T(8,128)(2,1)} %all-gather.4.cloned.1.call-done, bf16[1024,2048]{1,0:T(8,128)(2,1)} %param.7, f32[1024]{0:T(1024)S(1)} %add_rsqrt_fusion), kind=kOutput, calls=%fused_computation.5 | convolution fusion | flops 12891193344 | bytes 29364224 | tf_op jit(solution)/shard_map/dot_general | solution.py:37
  207.0 4.5 %fusion.5 = bf16[1,1024,192]{2,1,0:T(8,128)(2,1)S(1)} fusion(f32[1024]{0:T(1024)S(1)} %bitcast.47, pred[1024]{0:T(1024)(128)(4,1)S(1)} %get-tuple-element.19, pred[1024]{0:T(1024)(128)(4,1)S(1)} %get-tuple-element.18, pred[1024]{0:T(1024)(128)(4,1)S(1)} %get-tuple-element.17, pred[1024]{0:T(1024)(128)(4,1)S(1)} %get-tuple-element.16, ...), kind=kLoop, calls=%fused_computation.24 | loop fusion | flops 11206656 | bytes 12988416 | tf_op jit(solution)/shard_map/stack | solution.py:44
  211.5 4.5 %fusion.6 = bf16[1,1024,192]{2,1,0:T(8,128)(2,1)S(1)} fusion(f32[1024]{0:T(1024)S(1)} %bitcast.46, pred[1024]{0:T(1024)(128)(4,1)S(1)} %get-tuple-element.12, pred[1024]{0:T(1024)(128)(4,1)S(1)} %get-tuple-element.11, pred[1024]{0:T(1024)(128)(4,1)S(1)} %get-tuple-element.10, pred[1024]{0:T(1024)(128)(4,1)S(1)} %get-tuple-element.9, ...), kind=kLoop, calls=%fused_computation.25 | loop fusion | flops 11206656 | bytes 12988416 | tf_op jit(solution)/shard_map/stack | solution.py:44
  216.0 0.2 pad_maximum_fusion.1
  216.2 2.0 copy.22
  218.2 71.3 %all-gather.6.cloned.1.call-done = bf16[6144,512]{1,0:T(8,128)(2,1)} async-done(((bf16[768,512]{1,0:T(8,128)(2,1)}), bf16[6144,512]{1,0:T(8,128)(2,1)}) %all-gather.6.cloned.1.call-update) | async-done | bytes 6291472 | tf_op jit(solution)/shard_map/all_gather | solution.py:20
  289.5 1.2 constant_dynamic-slice_fusion
  290.8 1.2 copy.30
  292.0 0.5 broadcast.126
  292.5 5.4 %reduce.32 = bf16[768,512]{1,0:T(8,128)(2,1)S(1)} reduce(bf16[768,1,512]{2,1,0:T(2,128)(2,1)S(1)} %bitcast.37, bf16[]{:T(256)} %broadcast.126), dimensions={1}, to_apply=%bitcast.32.reduce_sub_computation | reduce | bytes 1572866
  297.9 1.4 reshape.117
  299.3 3.7 %all-to-all-start = ((bf16[4,2,49152]{2,1,0:T(2,128)(2,1)}), bf16[4,2,49152]{2,1,0:T(2,128)(2,1)S(1)}, u32[]{:S(2)}, u32[]{:S(2)}) async-start(bf16[4,2,49152]{2,1,0:T(2,128)(2,1)} %reshape.117), calls=%async_computation | async-start | bytes 1572864 | tf_op jit(solution)/shard_map/all_to_all | solution.py:67
  303.0 20.2 %all-to-all-done = bf16[4,2,49152]{2,1,0:T(2,128)(2,1)S(1)} async-done(((bf16[4,2,49152]{2,1,0:T(2,128)(2,1)}), bf16[4,2,49152]{2,1,0:T(2,128)(2,1)S(1)}, u32[]{:S(2)}, u32[]{:S(2)}) %all-to-all-start) | async-done | bytes 786464 | tf_op jit(solution)/shard_map/all_to_all | solution.py:67
  323.2 0.7 reshape.118
  324.0 0.2 copy.25
  324.2 1.0 copy.28
  325.2 2.7 dynamic-slice_bitcast_fusion
  327.9 7.8 %fusion.7 = (bf16[1,1024,768]{1,0,2:T(2,128)(2,1)S(1)}, bf16[1,1024,768]{1,0,2:T(2,128)(2,1)S(1)}) fusion(bf16[2,1024,768]{1,0,2:T(2,128)(2,1)} %all-gather.8.cloned.1.call-done), kind=kLoop, calls=%fused_computation.47 | loop fusion | bytes 6291456 | tf_op jit(solution)/shard_map/slice | solution.py:55
  335.7 0.6 copy.26
  336.3 0.6 copy.27
  336.9 1.9 select_select_fusion
  338.8 0.5 slice-done.1
  339.3 7.6 %convolution_convert_fusion = bf16[1024,512]{1,0:T(8,128)(2,1)} fusion(bf16[1024,6144]{0,1:T(8,128)(2,1)S(1)} %bitcast.33, bf16[6144,512]{1,0:T(8,128)(2,1)S(1)} %bitcast.45), kind=kOutput, calls=%fused_computation.10 | convolution fusion | flops 6442975232 | bytes 19922944 | tf_op jit(solution)/shard_map/dot_general | solution.py:57
  (20 shorter events, 0.1 us)
Async XLA Ops:
  7.2 3.8 %copy-start = (f32[8,96,512]{2,1,0:T(8,128)S(1)}, f32[8,96,512]{2,1,0:T(8,128)}, u32[]{:S(2)}) copy-start(f32[8,96,512]{2,1,0:T(8,128)} %param.11) | copy-start | bytes 4718596
  7.2 182.7 %all-gather.4.cloned.1.call-start = ((), (), s32[]{:S(2)}) async-start(), calls=%async_computation.1 | async-start | bytes 14155776 | tf_op jit(solution)/shard_map/all_gather | solution.py:19
  9.6 2.4 copy-start.2
  9.6 2.5 copy-start.1
  10.9 278.7 %all-gather.6.cloned.1.call-start = ((), (), s32[]{:S(2)}) async-start(), calls=%async_computation.2 | async-start | bytes 7077888 | tf_op jit(solution)/shard_map/all_gather | solution.py:20
  11.9 315.9 %all-gather.8.cloned.1.call-start = ((), (), s32[]{:S(2)}) async-start(), calls=%async_computation.3 | async-start | bytes 3932160 | tf_op jit(solution)/shard_map/all_gather | solution.py:45
  299.3 23.9 %all-to-all-start = ((bf16[4,2,49152]{2,1,0:T(2,128)(2,1)}), bf16[4,2,49152]{2,1,0:T(2,128)(2,1)S(1)}, u32[]{:S(2)}, u32[]{:S(2)}) async-start(bf16[4,2,49152]{2,1,0:T(2,128)(2,1)} %reshape.117), calls=%async_computation | async-start | bytes 1572864 | tf_op jit(solution)/shard_map/all_to_all | solution.py:67
  336.3 2.5 slice-start
  336.9 2.4 slice-start.1
Sparse Core Ops, SparseCore 0:
  11.0 178.8 all-gather.3
  192.6 96.8 all-gather.5
  291.7 35.1 all-gather.7
where the time goes:
time: 354 us; the launch traced here: 353 us
  waiting for transfers between devices  266 us (75%)
  matrix products  24.7 us (7%)
  other arithmetic  24.4 us (7%)
  local copies, waits for them, and re-layouts  20.5 us (6%)
  between operations  14 us (4%)
  starting transfers between devices  3.8 us (1%)
    all_gather x1, waiting for transfers between devices, on_device(): gate_up_all = lax.all_gather(gate_up, 'fs', axis=0, tiled=True)  175 us
    all_gather x1, waiting for transfers between devices, on_device(): lax.all_gather(down_train.astype(jnp.bfloat16).reshape(experts * down_row...  71.3 us
    all_to_all x1, waiting for transfers between devices, on_device(): lax.all_to_all(down_own, 'tp', split_axis=1, concat_axis=2, tiled=True)  20.2 us
    dot_general x1, matrix products, on_device(): acts = jnp.dot(normed, part, preferred_element_type=jnp.float32)  17.1 us
    another operation x3, other arithmetic, on_device(): jnp.stack([picked[k] * shares[:, k:k + 1] for k in range(picks)], 0)  9.18 us
    slice x1, local copies, waits for them, and re-layouts, on_device(): blocks[k]  7.82 us
    dot_general x1, matrix products, on_device(): jnp.dot(spread.reshape(tok_rows, group * depth), down_all[first * depth:(...  7.64 us
  transfers between devices with their start and end apart: 4, of which 3 were waited for; matrix products, arithmetic and copies ran while one was open for 13% of the time, Pallas kernels for 0%

commit v1 on v0

--- a/solution.py
+++ b/solution.py
@@ -4,6 +4,23 @@
 from jax.sharding import PartitionSpec as P
 
 epsilon = 1e-06
+
+
+def laid_out(blocks, dim):
+    shape = list(blocks.shape[1:])
+    shape[dim] *= blocks.shape[0]
+    return jnp.moveaxis(blocks, 0, dim).reshape(shape)
+
+
+def collect(x, axis, dim):
+    peers = lax.axis_size(axis)
+    right = [(i, (i + 1) % peers) for i in range(peers)]
+    parts = [x]
+    while len(parts) < peers:
+        parts.append(lax.ppermute(parts[-1], axis, right))
+    position = lax.axis_index(axis)
+    parts = jnp.stack(parts)[(position - jnp.arange(peers)) % peers]
+    return laid_out(parts, dim)
 
 
 def on_device(tokens, norm_gain, gate_train, up_train, down_train, expert_ids, route_weights):
@@ -16,7 +33,7 @@
         [norm_gain[None, :, None] * gate_train, norm_gain[None, :, None] * up_train], axis=2
     ).astype(jnp.bfloat16)
     gate_up = gate_up.transpose(1, 0, 2).reshape(rows, experts * 2 * cols)
-    gate_up_all = lax.all_gather(gate_up, "fs", axis=0, tiled=True)
+    gate_up_all = collect(gate_up, "fs", 0)
     down_all = lax.all_gather(
         down_train.astype(jnp.bfloat16).reshape(experts * down_rows, down_cols),
         "fs",

time: 354 us -> 445 us (1.26)
  waiting for transfers between devices: 266 us -> 322 us
  local copies, waits for them, and re-layouts: 20.5 us -> 53.7 us
    ppermute x0 -> x7, waiting for transfers between devices: none -> 309 us  [collect(): parts.append(lax.ppermute(parts[-1], axis, right))]
    all_gather x1 -> x0, waiting for transfers between devices: 175 us -> none  [on_device(): gate_up_all = lax.all_gather(gate_up, 'fs', axis=0, tiled=True)]
    all_gather x1, waiting for transfers between devices: 71.3 us -> 0.02 us  [on_device(): lax.all_gather(down_train.astype(jnp.bfloat16).reshape(experts * down_row...]
    unnamed x16 -> x33, local copies, waits for them, and re-layouts: 4.54 us -> 22.7 us
    gather x0 -> x1, local copies, waits for them, and re-layouts: none -> 11.1 us  [collect(): parts = jnp.stack(parts)[(position - jnp.arange(peers)) % peers]]
    all_to_all x1, waiting for transfers between devices: 20.2 us -> 13.2 us  [on_device(): lax.all_to_all(down_own, 'tp', split_axis=1, concat_axis=2, tiled=True)]
  transfers between devices with their start and end apart: 4 -> 10, of which waited for: 3 -> 8; matrix products, arithmetic and copies ran while one was open for 13% -> 17% of each run, Pallas kernels for 0% -> 0%
where the time goes in v1:
time: 445 us
  waiting for transfers between devices  322 us (72%)
  local copies, waits for them, and re-layouts  53.7 us (12%)
  matrix products  24.8 us (6%)
  other arithmetic  23.5 us (5%)
  between operations  14.3 us (3%)
  starting transfers between devices  6.61 us (1%)
    ppermute x7, waiting for transfers between devices, collect(): parts.append(lax.ppermute(parts[-1], axis, right))  309 us
    unnamed x33, local copies, waits for them, and re-layouts  22.7 us
    dot_general x1, matrix products, on_device(): acts = jnp.dot(normed, part, preferred_element_type=jnp.float32)  17.1 us
    all_to_all x1, waiting for transfers between devices, on_device(): lax.all_to_all(down_own, 'tp', split_axis=1, concat_axis=2, tiled=True)  13.2 us
    gather x1, local copies, waits for them, and re-layouts, collect(): parts = jnp.stack(parts)[(position - jnp.arange(peers)) % peers]  11.1 us
    another operation x3, other arithmetic, on_device(): jnp.stack([picked[k] * shares[:, k:k + 1] for k in range(picks)], 0)  9.27 us
  transfers between devices with their start and end apart: 10, of which 8 were waited for; matrix products, arithmetic and copies ran while one was open for 17% of the time, Pallas kernels for 0%

profile of v1, /device:TPU:0, one launch (start us, length us, event | category | flops | bytes accessed | tf_op | source)
XLA Modules:
  0.0 444.7 jit_solution(10951594704178108077)
XLA Ops:
  7.2 2.3 multiply_convert_fusion.1
  9.7 1.8 copy.38
  11.5 3.0 collective-permute-start
  14.5 37.6 %collective-permute-done = bf16[256,3072]{1,0:T(8,128)(2,1)S(1)} collective-permute-done((bf16[256,3072]{1,0:T(8,128)(2,1)}, bf16[256,3072]{1,0:T(8,128)(2,1)S(1)}, u32[]{:S(2)}, u32[]{:S(2)}) %collective-permute-start) | collective-permute-done | bytes 1572896 | tf_op jit(solution)/shard_map/ppermute | solution.py:20
  53.3 38.3 %collective-permute-done.1 = bf16[256,3072]{1,0:T(8,128)(2,1)S(1)} collective-permute-done((bf16[256,3072]{1,0:T(8,128)(2,1)S(1)}, bf16[256,3072]{1,0:T(8,128)(2,1)S(1)}, u32[]{:S(2)}, u32[]{:S(2)}) %collective-permute-start.1) | collective-permute-done | bytes 1572896 | tf_op jit(solution)/shard_map/ppermute | solution.py:20
  92.7 37.5 %collective-permute-done.2 = bf16[256,3072]{1,0:T(8,128)(2,1)} collective-permute-done((bf16[256,3072]{1,0:T(8,128)(2,1)S(1)}, bf16[256,3072]{1,0:T(8,128)(2,1)}, u32[]{:S(2)}, u32[]{:S(2)}) %collective-permute-start.2) | collective-permute-done | bytes 1572896 | tf_op jit(solution)/shard_map/ppermute | solution.py:20
  131.3 61.2 %collective-permute-done.3 = bf16[256,3072]{1,0:T(8,128)(2,1)} collective-permute-done((bf16[256,3072]{1,0:T(8,128)(2,1)}, bf16[256,3072]{1,0:T(8,128)(2,1)}, u32[]{:S(2)}, u32[]{:S(2)}) %collective-permute-start.3) | collective-permute-done | bytes 1572896 | tf_op jit(solution)/shard_map/ppermute | solution.py:20
  193.7 3.2 fusion
  196.9 1.3 constant_dynamic-update-slice_fusion
  198.2 63.2 %collective-permute-done.4 = bf16[256,3072]{1,0:T(8,128)(2,1)} collective-permute-done((bf16[256,3072]{1,0:T(8,128)(2,1)}, bf16[256,3072]{1,0:T(8,128)(2,1)}, u32[]{:S(2)}, u32[]{:S(2)}) %collective-permute-start.4) | collective-permute-done | bytes 1572896 | tf_op jit(solution)/shard_map/ppermute | solution.py:20
  261.3 1.2 bitcast_dynamic-update-slice_fusion.6
  262.6 1.2 bitcast_dynamic-update-slice_fusion.5
  263.8 2.7 bitcast_dynamic-update-slice_fusion.4
  266.5 45.3 %collective-permute-done.5 = bf16[256,3072]{1,0:T(8,128)(2,1)S(1)} collective-permute-done((bf16[256,3072]{1,0:T(8,128)(2,1)}, bf16[256,3072]{1,0:T(8,128)(2,1)S(1)}, u32[]{:S(2)}, u32[]{:S(2)}) %collective-permute-start.5) | collective-permute-done | bytes 1572896 | tf_op jit(solution)/shard_map/ppermute | solution.py:20
  311.8 2.7 bitcast_dynamic-update-slice_fusion.3
  314.5 2.7 bitcast_dynamic-update-slice_fusion.2
  317.2 1.3 bitcast_dynamic-update-slice_fusion.1
  318.5 25.5 %collective-permute-done.6 = bf16[256,3072]{1,0:T(8,128)(2,1)S(1)} collective-permute-done((bf16[256,3072]{1,0:T(8,128)(2,1)S(1)}, bf16[256,3072]{1,0:T(8,128)(2,1)S(1)}, u32[]{:S(2)}, u32[]{:S(2)}) %collective-permute-start.6) | collective-permute-done | bytes 1572896 | tf_op jit(solution)/shard_map/ppermute | solution.py:20
  345.2 11.1 %gather_fusion = bf16[8,256,3072]{2,1,0:T(8,128)(2,1)} fusion(bf16[8,256,3072]{2,1,0:T(8,128)(2,1)} %bitcast_dynamic-update-slice_fusion, s32[1024]{0:T(1024)S(1)} %pad_clamp_fusion), kind=kCustom, calls=%fused_computation | custom fusion | bytes 25165856 | tf_op jit(solution)/shard_map/gather | solution.py:22
  356.3 17.1 %fusion.2 = f32[1024,3072]{1,0:T(8,128)S(1)} fusion(bf16[2048,3072]{1,0:T(8,128)(2,1)} %bitcast.50, bf16[1024,2048]{1,0:T(8,128)(2,1)} %param.7, f32[1024]{0:T(1024)S(1)} %add_rsqrt_fusion), kind=kOutput, calls=%fused_computation.6 | convolution fusion | flops 12891193344 | bytes 29364224 | tf_op jit(solution)/shard_map/dot_general | solution.py:54
  373.4 4.5 %fusion.5 = bf16[1,1024,192]{2,1,0:T(8,128)(2,1)S(1)} fusion(f32[1024]{0:T(1024)S(1)} %bitcast.69, pred[1024]{0:T(1024)(128)(4,1)S(1)} %get-tuple-element.19, pred[1024]{0:T(1024)(128)(4,1)S(1)} %get-tuple-element.18, pred[1024]{0:T(1024)(128)(4,1)S(1)} %get-tuple-element.17, pred[1024]{0:T(1024)(128)(4,1)S(1)} %get-tuple-element.16, ...), kind=kLoop, calls=%fused_computation.30 | loop fusion | flops 11206656 | bytes 12988416 | tf_op jit(solution)/shard_map/stack | solution.py:61
  378.0 4.5 %fusion.6 = bf16[1,1024,192]{2,1,0:T(8,128)(2,1)S(1)} fusion(f32[1024]{0:T(1024)S(1)} %bitcast.68, pred[1024]{0:T(1024)(128)(4,1)S(1)} %get-tuple-element.12, pred[1024]{0:T(1024)(128)(4,1)S(1)} %get-tuple-element.11, pred[1024]{0:T(1024)(128)(4,1)S(1)} %get-tuple-element.10, pred[1024]{0:T(1024)(128)(4,1)S(1)} %get-tuple-element.9, ...), kind=kLoop, calls=%fused_computation.31 | loop fusion | flops 11206656 | bytes 12988416 | tf_op jit(solution)/shard_map/stack | solution.py:61
  382.7 2.0 copy.34
  387.8 5.4 %reduce.32 = bf16[768,512]{1,0:T(8,128)(2,1)S(1)} reduce(bf16[768,1,512]{2,1,0:T(2,128)(2,1)S(1)} %bitcast.57, bf16[]{:T(256)} %broadcast.195), dimensions={1}, to_apply=%bitcast.49.reduce_sub_computation | reduce | bytes 1572866
  393.2 1.6 reshape.178
  394.8 3.5 all-to-all-start
  398.4 3.0 constant_dynamic-slice_fusion.2
  401.4 1.2 copy.41
  403.9 13.2 %all-to-all-done = bf16[4,2,49152]{2,1,0:T(2,128)(2,1)S(1)} async-done(((bf16[4,2,49152]{2,1,0:T(2,128)(2,1)}), bf16[4,2,49152]{2,1,0:T(2,128)(2,1)S(1)}, u32[]{:S(2)}, u32[]{:S(2)}) %all-to-all-start) | async-done | bytes 786464 | tf_op jit(solution)/shard_map/all_to_all | solution.py:84
  419.0 7.6 %fusion.9 = (bf16[1,1024,768]{1,0,2:T(2,128)(2,1)S(1)}, bf16[1,1024,768]{1,0,2:T(2,128)(2,1)S(1)}) fusion(bf16[2,1024,768]{1,0,2:T(2,128)(2,1)} %all-gather.5.cloned.1.call-done), kind=kLoop, calls=%fused_computation.63 | loop fusion | bytes 6291456 | tf_op jit(solution)/shard_map/slice | solution.py:72
  427.8 1.9 select_select_fusion
  430.2 7.6 %convolution_convert_fusion = bf16[1024,512]{1,0:T(8,128)(2,1)} fusion(bf16[1024,6144]{0,1:T(8,128)(2,1)S(1)} %bitcast.54, bf16[6144,512]{1,0:T(8,128)(2,1)S(1)} %bitcast.67), kind=kOutput, calls=%fused_computation.18 | convolution fusion | flops 6442975232 | bytes 19922944 | tf_op jit(solution)/shard_map/dot_general | solution.py:74
  (54 shorter events, 14.0 us)
Async XLA Ops:
  7.2 123.0 %copy-start = (f32[8,96,512]{2,1,0:T(8,128)S(1)}, f32[8,96,512]{2,1,0:T(8,128)}, u32[]{:S(2)}) copy-start(f32[8,96,512]{2,1,0:T(8,128)} %param.11) | copy-start | bytes 4718596
  7.2 377.6 %all-gather.3.cloned.1.call-start = ((), (), s32[]{:S(2)}) async-start(), calls=%async_computation.1 | async-start | bytes 7077888 | tf_op jit(solution)/shard_map/all_gather | solution.py:37
  9.6 183.8 %copy-start.6 = (f32[1024,2]{0,1:T(2,128)S(1)}, f32[1024,2]{0,1:T(2,128)}, u32[]{:S(2)}) copy-start(f32[1024,2]{0,1:T(2,128)} %param.13) | copy-start | bytes 24580
  9.6 183.9 %copy-start.5 = (s32[1024,2]{0,1:T(2,128)S(1)}, s32[1024,2]{0,1:T(2,128)}, u32[]{:S(2)}) copy-start(s32[1024,2]{0,1:T(2,128)} %param.12) | copy-start | bytes 24580
  11.5 40.6 %collective-permute-start = (bf16[256,3072]{1,0:T(8,128)(2,1)}, bf16[256,3072]{1,0:T(8,128)(2,1)S(1)}, u32[]{:S(2)}, u32[]{:S(2)}) collective-permute-start(bf16[256,3072]{1,0:T(8,128)(2,1)} %copy.38), channel_id=1, source_target_pairs={{0,4},{4,8},{8,12},{12,16},{16,20},{20,24},{24,28},{28,0},{1,5},{5... | collective-permute-start | bytes 4718600 | tf_op jit(solution)/shard_map/ppermute | solution.py:20
  52.1 1.2 copy-start.1
  53.3 38.3 %collective-permute-start.1 = (bf16[256,3072]{1,0:T(8,128)(2,1)S(1)}, bf16[256,3072]{1,0:T(8,128)(2,1)S(1)}, u32[]{:S(2)}, u32[]{:S(2)}) collective-permute-start(bf16[256,3072]{1,0:T(8,128)(2,1)S(1)} %collective-permute-done), channel_id=1, source_target_pairs={{0,4},{4,8},{8,12},{12,16},{16,20},{20,24},{24,28},{28,0},{1,5},{5... | collective-permute-start | bytes 4718600 | tf_op jit(solution)/shard_map/ppermute | solution.py:20
  91.5 1.2 copy-start.3
  92.7 37.5 %collective-permute-start.2 = (bf16[256,3072]{1,0:T(8,128)(2,1)S(1)}, bf16[256,3072]{1,0:T(8,128)(2,1)}, u32[]{:S(2)}, u32[]{:S(2)}) collective-permute-start(bf16[256,3072]{1,0:T(8,128)(2,1)S(1)} %collective-permute-done.1), channel_id=1, source_target_pairs={{0,4},{4,8},{8,12},{12,16},{16,20},{20,24},{24,28},{28,0},{1,5},{5... | collective-permute-start | bytes 4718600 | tf_op jit(solution)/shard_map/ppermute | solution.py:20
  130.2 62.3 %collective-permute-start.3 = (bf16[256,3072]{1,0:T(8,128)(2,1)}, bf16[256,3072]{1,0:T(8,128)(2,1)}, u32[]{:S(2)}, u32[]{:S(2)}) collective-permute-start(bf16[256,3072]{1,0:T(8,128)(2,1)} %collective-permute-done.2), channel_id=1, source_target_pairs={{0,4},{4,8},{8,12},{12,16},{16,20},{20,24},{24,28},{28,0},{1,5},{5... | collective-permute-start | bytes 4718600 | tf_op jit(solution)/shard_map/ppermute | solution.py:20
  131.2 287.8 %all-gather.5.cloned.1.call-start = ((), (), s32[]{:S(2)}) async-start(), calls=%async_computation.2 | async-start | bytes 3932160 | tf_op jit(solution)/shard_map/all_gather | solution.py:62
  192.5 68.8 %collective-permute-start.4 = (bf16[256,3072]{1,0:T(8,128)(2,1)}, bf16[256,3072]{1,0:T(8,128)(2,1)}, u32[]{:S(2)}, u32[]{:S(2)}) collective-permute-start(bf16[256,3072]{1,0:T(8,128)(2,1)} %collective-permute-done.3), channel_id=1, source_target_pairs={{0,4},{4,8},{8,12},{12,16},{16,20},{20,24},{24,28},{28,0},{1,5},{5... | collective-permute-start | bytes 4718600 | tf_op jit(solution)/shard_map/ppermute | solution.py:20
  193.4 67.9 %copy-start.2 = (bf16[256,3072]{1,0:T(8,128)(2,1)S(1)}, bf16[256,3072]{1,0:T(8,128)(2,1)}, u32[]{:S(2)}) copy-start(bf16[256,3072]{1,0:T(8,128)(2,1)} %copy-done.1) | copy-start | bytes 4718596
  193.5 69.1 %copy-start.4 = (bf16[256,3072]{1,0:T(8,128)(2,1)S(1)}, bf16[256,3072]{1,0:T(8,128)(2,1)}, u32[]{:S(2)}) copy-start(bf16[256,3072]{1,0:T(8,128)(2,1)} %copy-done.3) | copy-start | bytes 4718596
  261.3 50.5 %collective-permute-start.5 = (bf16[256,3072]{1,0:T(8,128)(2,1)}, bf16[256,3072]{1,0:T(8,128)(2,1)S(1)}, u32[]{:S(2)}, u32[]{:S(2)}) collective-permute-start(bf16[256,3072]{1,0:T(8,128)(2,1)} %collective-permute-done.4), channel_id=1, source_target_pairs={{0,4},{4,8},{8,12},{12,16},{16,20},{20,24},{24,28},{28,0},{1,5},{5... | collective-permute-start | bytes 4718600 | tf_op jit(solution)/shard_map/ppermute | solution.py:20
  311.8 32.2 %collective-permute-start.6 = (bf16[256,3072]{1,0:T(8,128)(2,1)S(1)}, bf16[256,3072]{1,0:T(8,128)(2,1)S(1)}, u32[]{:S(2)}, u32[]{:S(2)}) collective-permute-start(bf16[256,3072]{1,0:T(8,128)(2,1)S(1)} %collective-permute-done.5), channel_id=1, source_target_pairs={{0,4},{4,8},{8,12},{12,16},{16,20},{20,24},{24,28},{28,0},{1,5},{5... | collective-permute-start | bytes 4718600 | tf_op jit(solution)/shard_map/ppermute | solution.py:20
  394.8 22.3 %all-to-all-start = ((bf16[4,2,49152]{2,1,0:T(2,128)(2,1)}), bf16[4,2,49152]{2,1,0:T(2,128)(2,1)S(1)}, u32[]{:S(2)}, u32[]{:S(2)}) async-start(bf16[4,2,49152]{2,1,0:T(2,128)(2,1)} %reshape.178), calls=%async_computation | async-start | bytes 1572864 | tf_op jit(solution)/shard_map/all_to_all | solution.py:84
  427.2 2.5 slice-start
  427.8 2.4 slice-start.1
Sparse Core Ops, SparseCore 0:
  131.3 152.6 all-gather.2
  384.9 32.4 all-gather.4
